TPU v7x, 32 devices: a whole 2x2x4 slice. The times are simulated.
32 devices in a mesh: kv: 8 (over z, y), tp: 4 (over x, core).
Axes of the slice: x: 2, y: 2, z: 4, core: 2. Of those that a mesh axis runs over, the one named last changes fastest.
Arguments:
- piece_tokens: bfloat16 [32, 2048], P('kv'), may hold values from -6 to 6
- decode_tokens: bfloat16 [8, 2048], P('kv'), may hold values from -6 to 6
- prompt_fill: int32 [1], replicated, may hold values from 1024 to 2016
- decode_fill: int32 [8], P('kv'), may hold values from 1 to 767, 3072 in all
- prompt_cache: bfloat16 [2048, 544], P('kv'), may hold values from -600 to 600
- decode_cache: bfloat16 [8, 768, 544], P('kv'), may hold values from -600 to 600
- input_gain: float32 [2048], replicated, may hold values from 0.1 to 1.9
- query_gain: float32 [768], replicated, may hold values from 0.1 to 1.9
- latent_gain: float32 [512], replicated, may hold values from 0.1 to 1.9
- query_down: bfloat16 [2048, 768], P(None, 'tp'), may hold values from -0.125 to 0.125
- latent_down: bfloat16 [2048, 512], P(None, 'tp'), may hold values from -0.125 to 0.125
- rope_down: bfloat16 [2048, 32], replicated, may hold values from -0.125 to 0.125
- query_up: bfloat16 [768, 1024], P(None, 'tp'), may hold values from -0.21875 to 0.21875
- qrope_up: bfloat16 [768, 512], P(None, 'tp'), may hold values from -0.21875 to 0.21875
- key_up: bfloat16 [16, 64, 512], P('tp'), may hold values from -0.25 to 0.25
- value_up: bfloat16 [16, 512, 64], P('tp'), may hold values from -4 to 4
- out_proj: bfloat16 [1024, 2048], P('tp'), may hold values from -4 to 4
Outputs:
- piece_out: bfloat16 [32, 2048], P('kv')
- decode_out: bfloat16 [8, 2048], P('kv')
- piece_rows: bfloat16 [32, 544], P('kv')
- decode_rows: bfloat16 [8, 544], P('kv')
Inputs may be any that keep to these rules, and one draw needn't show every extreme that they name: `prompt_fill`: the piece takes the 32 positions that follow the cache's filled positions. `decode_fill`: a decoding sequence's new token takes the position that follows its filled ones.
All inputs are finite; a program needn't handle non-finite values. No bound on the sum of `decode_fill` on one device may be relied on, other than what follows from the above.
Results may differ from a plain program's by a relative error of at most 0.035.
Values may be sent and summed in bfloat16 or wider, within the bound.
A program may use at most 64 MiB of HBM per device.

v0:
```python
import jax
import jax.numpy as jnp
from jax import lax
from jax.sharding import PartitionSpec as P

NOPE = 64
ROPE = 32
NEG_FILL = -1e30
RMS_EPS = 1e-06
THETA = 10000.0


def rms_scale(values, gain_row):
    widened = values.astype(jnp.float32)
    scaled = (
        widened
        * lax.rsqrt(jnp.mean(widened * widened, axis=-1, keepdims=True) + RMS_EPS)
        * gain_row
    )
    return scaled.astype(jnp.bfloat16)


def rotate(values, places):
    half_width = values.shape[-1] // 2
    inverse = THETA ** (-jnp.arange(half_width, dtype=jnp.float32) / half_width)
    angles = places.astype(jnp.float32)[..., None] * inverse
    first_half = values[..., :half_width].astype(jnp.float32)
    second_half = values[..., half_width:].astype(jnp.float32)
    cosine = jnp.cos(angles)
    sine_part = jnp.sin(angles)
    return jnp.concatenate(
        [
            first_half * cosine - second_half * sine_part,
            first_half * sine_part + second_half * cosine,
        ],
        axis=-1,
    ).astype(jnp.bfloat16)


def make_queries(query_lat, places, query_up, qrope_up, key_up):
    row_count = query_lat.shape[0]
    head_count = key_up.shape[0]
    nope_part = (
        jnp.dot(query_lat, query_up, preferred_element_type=jnp.float32)
        .astype(jnp.bfloat16)
        .reshape(row_count, head_count, -1)
    )
    rope_raw = (
        jnp.dot(query_lat, qrope_up, preferred_element_type=jnp.float32)
        .astype(jnp.bfloat16)
        .reshape(row_count, head_count, -1)
    )
    turned = rotate(rope_raw, places[:, None])
    absorbed = jnp.einsum(
        "nhc,hcl->nhl", nope_part, key_up, preferred_element_type=jnp.float32
    ).astype(jnp.bfloat16)
    return (absorbed, turned)


def block_attend(absorbed, turned, key_rows, key_places, query_places, value_up):
    latent_width = value_up.shape[1]
    score_scale = (NOPE + ROPE) ** (-0.5)
    latent_keys = key_rows[:, :latent_width]
    scores = (
        jnp.einsum("nhl,sl->nhs", absorbed, latent_keys, preferred_element_type=jnp.float32)
        + jnp.einsum(
            "nhr,sr->nhs", turned, key_rows[:, latent_width:], preferred_element_type=jnp.float32
        )
    ) * score_scale
    allowed = key_places[None, None, :] <= query_places[:, None, None]
    scores = jnp.where(allowed, scores, NEG_FILL)
    local_peak = jnp.max(scores, axis=-1)
    exp_scores = jnp.where(allowed, jnp.exp(scores - local_peak[..., None]), 0.0)
    weight_sum = jnp.sum(exp_scores, axis=-1)
    weights = exp_scores.astype(jnp.bfloat16)
    mixed_rows = jnp.einsum("nhs,sl->nhl", weights, latent_keys, preferred_element_type=jnp.float32)
    partial_sum = jnp.einsum(
        "nhl,hlv->nhv", mixed_rows, value_up.astype(jnp.float32), precision=lax.Precision.HIGHEST
    )
    return (partial_sum, weight_sum, local_peak)


def insert_row(cache_rows, new_row, fill_one):
    return lax.dynamic_update_slice(cache_rows, new_row[None], (fill_one, jnp.zeros((), jnp.int32)))


def local(
    piece_tokens,
    decode_tokens,
    prompt_fill,
    decode_fill,
    prompt_cache,
    decode_cache,
    input_gain,
    query_gain,
    latent_gain,
    query_down,
    latent_down,
    rope_down,
    query_up,
    qrope_up,
    key_up,
    value_up,
    out_proj,
):
    kv_index = lax.axis_index("kv")
    piece_dev = piece_tokens.shape[0]
    shard_len = prompt_cache.shape[0]
    fill_start = prompt_fill[0]
    own_places = fill_start + kv_index * piece_dev + jnp.arange(piece_dev, dtype=jnp.int32)
    places = jnp.concatenate([own_places, decode_fill])
    tokens = jnp.concatenate([piece_tokens, decode_tokens], axis=0)
    normed = rms_scale(tokens, input_gain)
    query_comp = jnp.dot(normed, query_down, preferred_element_type=jnp.float32).astype(
        jnp.bfloat16
    )
    latent_comp = jnp.dot(normed, latent_down, preferred_element_type=jnp.float32).astype(
        jnp.bfloat16
    )
    query_comp, latent_comp = (
        lax.all_gather(query_comp, "tp", axis=1, tiled=True),
        lax.all_gather(latent_comp, "tp", axis=1, tiled=True),
    )
    query_lat = rms_scale(query_comp, query_gain)
    rope_raw = jnp.dot(normed, rope_down, preferred_element_type=jnp.float32).astype(jnp.bfloat16)
    new_rows = jnp.concatenate(
        [rms_scale(latent_comp, latent_gain), rotate(rope_raw, places)], axis=-1
    )
    piece_rows = new_rows[:piece_dev]
    decode_rows = new_rows[piece_dev:]
    decode_absorbed, decode_turned = make_queries(
        query_lat[piece_dev:], decode_fill, query_up, qrope_up, key_up
    )
    piece_latent, arrived = (
        lax.all_gather(query_lat[:piece_dev], "kv", axis=0, tiled=True),
        lax.all_gather(piece_rows, "kv", axis=0, tiled=True),
    )
    arrived_places = fill_start + jnp.arange(arrived.shape[0], dtype=jnp.int32)
    piece_absorbed, piece_turned = make_queries(
        piece_latent, arrived_places, query_up, qrope_up, key_up
    )
    piece_total = arrived.shape[0]
    query_places = fill_start + jnp.arange(piece_total, dtype=jnp.int32)
    zero_rows = jnp.zeros((shard_len, arrived.shape[1]), arrived.dtype)
    padded = jnp.concatenate([zero_rows, arrived, zero_rows], axis=0)
    offset = jnp.clip(kv_index * shard_len - fill_start + shard_len, 0, piece_total + shard_len)
    window = lax.dynamic_slice_in_dim(padded, offset, shard_len, 0)
    key_places = kv_index * shard_len + jnp.arange(shard_len, dtype=jnp.int32)
    fresh_rows = (key_places >= fill_start) & (key_places < fill_start + piece_total)
    key_rows = jnp.where(fresh_rows[:, None], window, prompt_cache)
    partial_sum, weight_sum, local_peak = block_attend(
        piece_absorbed, piece_turned, key_rows, key_places, query_places, value_up
    )
    all_parts, all_totals, all_peaks = (
        lax.all_to_all(
            partial_sum.reshape(1, piece_total, -1), "kv", split_axis=1, concat_axis=0, tiled=True
        ),
        lax.all_to_all(weight_sum[None], "kv", split_axis=1, concat_axis=0, tiled=True),
        lax.all_to_all(local_peak[None], "kv", split_axis=1, concat_axis=0, tiled=True),
    )
    global_peak = jnp.max(all_peaks, axis=0)
    factor = jnp.exp(all_peaks - global_peak[None])
    merged = jnp.sum(all_parts.reshape(all_peaks.shape + (-1,)) * factor[..., None], axis=0)
    denominator = jnp.sum(all_totals * factor, axis=0)
    piece_value = (merged / denominator[..., None]).astype(jnp.bfloat16)
    decode_keys = jax.vmap(insert_row)(decode_cache, decode_rows, decode_fill)

    def attend_one(absorbed_one, turned_one, keys_one, fill_one):
        cache_places = jnp.arange(keys_one.shape[0], dtype=jnp.int32)
        return block_attend(
            absorbed_one[None], turned_one[None], keys_one, cache_places, fill_one[None], value_up
        )

    decode_part, decode_total, decode_peak = jax.vmap(attend_one)(
        decode_absorbed, decode_turned, decode_keys, decode_fill
    )
    decode_value = (decode_part[:, 0] / decode_total[:, 0, :, None]).astype(jnp.bfloat16)
    values = jnp.concatenate([piece_value, decode_value], axis=0)
    values = values.reshape(values.shape[0], -1)
    partial_value = jnp.dot(values, out_proj, preferred_element_type=jnp.float32).astype(
        jnp.bfloat16
    )
    summed = lax.psum(partial_value, "tp").astype(jnp.float32).astype(jnp.bfloat16)
    return (summed[:piece_dev], summed[piece_dev:], piece_rows, decode_rows)


def solution(mesh):
    placed = (
        P("kv", None),
        P("kv", None),
        P(),
        P("kv"),
        P("kv", None),
        P("kv", None, None),
        P(),
        P(),
        P(),
        P(None, "tp"),
        P(None, "tp"),
        P(),
        P(None, "tp"),
        P(None, "tp"),
        P("tp", None, None),
        P("tp", None, None),
        P("tp", None),
    )
    return jax.shard_map(
        local,
        mesh=mesh,
        in_specs=placed,
        out_specs=(P("kv", None), P("kv", None), P("kv", None), P("kv", None)),
        check_vma=False,
    )
```

profile of v0, /device:TPU:0, one launch (start us, length us, event | category | flops | bytes accessed | tf_op | source)
XLA Modules:
  0.0 135.7 jit_solution(8345209168863359578)
XLA Ops:
  0.7 1.3 copy.80
  4.0 6.2 %all_gather.14 = bf16[5,512]{1,0:T(8,128)(2,1)S(1)} all-gather(bf16[5,128]{1,0:T(8,128)(2,1)S(1)} %convolution_convert_fusion.5), channel_id=1, replica_groups=mesh['kv'=8,'tp'=4] {'tp'}, dimensions={1}, use_global_device_ids=true | all-gather | bytes 6400 | tf_op jit(solution)/shard_map/all_gather | solution.py:122
  10.6 5.5 %all-gather = bf16[4,192,5]{1,2,0:T(8,128)(2,1)S(1)} all-gather(bf16[1,192,5]{1,2,0:T(8,128)(2,1)S(1)} %fusion.5), channel_id=1, replica_groups=mesh['kv'=8,'tp'=4] {'tp'}, dimensions={0}, use_global_device_ids=true | all-gather | bytes 9600 | tf_op jit(solution)/shard_map/all_gather | solution.py:121
  17.6 31.4 %all-gather.2 = bf16[8,4,544]{2,1,0:T(4,128)(2,1)S(1)} all-gather(bf16[1,4,544]{2,1,0:T(4,128)(2,1)S(1)} %slice_bitcast_fusion.14), channel_id=1, replica_groups=mesh['kv'=8,'tp'=4] {'kv'}, dimensions={0}, use_global_device_ids=true | all-gather | bytes 39168 | tf_op jit(solution)/shard_map/all_gather | solution.py:136
  49.2 30.8 %all-gather.1 = bf16[8,4,768]{2,1,0:T(4,128)(2,1)S(1)} all-gather(bf16[1,4,768]{2,1,0:T(4,128)(2,1)S(1)} %slice_bitcast_fusion.10), channel_id=1, replica_groups=mesh['kv'=8,'tp'=4] {'kv'}, dimensions={0}, use_global_device_ids=true | all-gather | bytes 55296 | tf_op jit(solution)/shard_map/all_gather | solution.py:135
  80.9 0.9 fusion.10
  81.9 0.7 copy-done.2
  83.2 0.7 copy.46
  83.9 5.4 %all-to-all-start.2 = ((f32[1,32,4]{2,0,1:T(1,128)}), f32[1,32,4]{2,0,1:T(1,128)S(1)}, u32[]{:S(2)}, u32[]{:S(2)}) async-start(f32[1,32,4]{2,0,1:T(1,128)} %copy.46), calls=%async_computation.2 | async-start | bytes 32768 | tf_op jit(solution)/shard_map/all_to_all | solution.py:158
  89.9 0.6 copy-done.14
  91.3 0.8 constant_dynamic-slice_fusion
  92.1 0.7 copy-done.13
  92.8 2.0 %and_reduce_fusion = pred[]{:T(512)} fusion(s32[3]{0:T(128)S(1)} %copy-done.13, s32[1]{0:T(128)} %bitcast.20, s32[1]{0:T(128)} %bitcast.19, s32[1]{0:T(128)} %constant.79.clone.1), kind=kLoop, calls=%fused_computation.108 | loop fusion | flops 17 | bytes 25 | tf_op jit(solution)/shard_map/reduce.1
  94.8 1.2 broadcast_select_fusion
  96.2 1.6 %scatter.4 = bf16[1,768,544]{1,2,0:T(8,128)(2,1)S(1)} dynamic-update-slice(bf16[1,768,544]{1,2,0:T(8,128)(2,1)S(1)} %copy.80, bf16[1,1,544]{1,2,0:T(8,128)(2,1)S(1)} %copy.50, s32[]{:T(128)} %constant.75.clone.1, s32[]{:T(128)} %bitcast.22, s32[]{:T(128)} %constant.75.clone.1) | dynamic-update-slice | bytes 2180 | tf_op jit(solution)/shard_map/vmap(vmap())/scatter | solution.py:84
  99.1 0.6 copy-done.7
  100.6 0.7 copy.43
  101.3 6.0 %all-to-all-start.1 = ((f32[1,32,4]{2,0,1:T(1,128)}), f32[1,32,4]{2,0,1:T(1,128)S(1)}, u32[]{:S(2)}, u32[]{:S(2)}) async-start(f32[1,32,4]{2,0,1:T(1,128)} %copy.43), calls=%async_computation.1 | async-start | bytes 32768 | tf_op jit(solution)/shard_map/all_to_all | solution.py:159
  108.1 0.7 reshape.442
  109.0 4.9 %all-to-all-done.1 = f32[1,32,4]{2,0,1:T(1,128)S(1)} async-done(((f32[1,32,4]{2,0,1:T(1,128)}), f32[1,32,4]{2,0,1:T(1,128)S(1)}, u32[]{:S(2)}, u32[]{:S(2)}) %all-to-all-start.1) | async-done | bytes 544 | tf_op jit(solution)/shard_map/all_to_all | solution.py:159
  113.9 3.3 %all-to-all-start = ((f32[1,32,256]{2,0,1:T(1,128)}), f32[1,32,256]{2,0,1:T(1,128)S(1)}, u32[]{:S(2)}, u32[]{:S(2)}) async-start(f32[1,32,256]{2,0,1:T(1,128)} %reshape.442), calls=%async_computation | async-start | bytes 65536 | tf_op jit(solution)/shard_map/all_to_all | solution.py:155
  118.1 5.7 %all-to-all-done = f32[1,32,256]{2,0,1:T(1,128)S(1)} async-done(((f32[1,32,256]{2,0,1:T(1,128)}), f32[1,32,256]{2,0,1:T(1,128)S(1)}, u32[]{:S(2)}, u32[]{:S(2)}) %all-to-all-start) | async-done | bytes 32800 | tf_op jit(solution)/shard_map/all_to_all | solution.py:155
  124.2 10.3 %psum.7 = bf16[5,2048]{1,0:T(8,128)(2,1)S(1)} all-reduce(bf16[5,2048]{1,0:T(8,128)(2,1)S(1)} %convolution_convert_fusion), channel_id=1, replica_groups=mesh['kv'=8,'tp'=4] {'tp'}, use_global_device_ids=true, to_apply=%region_11.12 | all-reduce | flops 10240 | bytes 40960 | tf_op jit(solution)/shard_map/psum | solution.py:183
  134.5 0.6 slice.104
  (107 shorter events, 10.6 us)
Async XLA Ops:
  0.6 123.3 %copy-start = (bf16[256,2048]{1,0:T(8,128)(2,1)S(1)}, bf16[256,2048]{1,0:T(8,128)(2,1)}, u32[]{:S(2)}) copy-start(bf16[256,2048]{1,0:T(8,128)(2,1)} %param.35) | copy-start | bytes 3145732
  0.6 3.1 %copy-start.5 = (bf16[2048,128]{1,0:T(8,128)(2,1)S(1)}, bf16[2048,128]{1,0:T(8,128)(2,1)}, u32[]{:S(2)}) copy-start(bf16[2048,128]{1,0:T(8,128)(2,1)} %param.29) | copy-start | bytes 1572868
  0.7 2.9 %copy-start.15 = (bf16[2048,32]{0,1:T(8,128)(2,1)S(1)}, bf16[2048,32]{0,1:T(8,128)(2,1)}, u32[]{:S(2)}) copy-start(bf16[2048,32]{0,1:T(8,128)(2,1)} %param.30) | copy-start | bytes 393220
  0.7 2.7 %copy-start.8 = (bf16[4,2048]{1,0:T(4,128)(2,1)S(1)}, bf16[4,2048]{1,0:T(4,128)(2,1)}, u32[]{:S(2)}) copy-start(bf16[4,2048]{1,0:T(4,128)(2,1)} %param.19) | copy-start | bytes 49156
  0.7 2.7 %copy-start.9 = (bf16[1,2048]{1,0:T(2,128)(2,1)S(1)}, bf16[1,2048]{1,0:T(2,128)(2,1)}, u32[]{:S(2)}) copy-start(bf16[1,2048]{1,0:T(2,128)(2,1)} %param.20) | copy-start | bytes 12292
  0.7 2.9 %copy-start.10 = (f32[2048]{0:T(1024)S(1)}, f32[2048]{0:T(1024)}, u32[]{:S(2)}) copy-start(f32[2048]{0:T(1024)} %param.25) | copy-start | bytes 24580
  2.0 8.3 %copy-start.3 = (bf16[2048,192]{0,1:T(8,128)(2,1)S(1)}, bf16[2048,192]{0,1:T(8,128)(2,1)}, u32[]{:S(2)}) copy-start(bf16[2048,192]{0,1:T(8,128)(2,1)} %param.28) | copy-start | bytes 2359300
  10.3 6.1 %copy-start.6 = (bf16[256,544]{0,1:T(8,128)(2,1)S(1)}, bf16[256,544]{0,1:T(8,128)(2,1)}, u32[]{:S(2)}) copy-start(bf16[256,544]{0,1:T(8,128)(2,1)} %param.23) | copy-start | bytes 835588
  16.6 0.7 copy-start.12
  17.3 31.8 %copy-start.11 = (f32[768]{0:T(1024)S(1)}, f32[768]{0:T(1024)}, u32[]{:S(2)}) copy-start(f32[768]{0:T(1024)} %param.26) | copy-start | bytes 9220
  17.5 62.5 %copy-start.4 = (bf16[768,128]{1,0:T(8,128)(2,1)S(1)}, bf16[768,128]{1,0:T(8,128)(2,1)}, u32[]{:S(2)}) copy-start(bf16[768,128]{1,0:T(8,128)(2,1)} %param.32) | copy-start | bytes 589828
  17.5 62.8 %copy-start.1 = (bf16[768,256]{1,0:T(8,128)(2,1)S(1)}, bf16[768,256]{1,0:T(8,128)(2,1)}, u32[]{:S(2)}) copy-start(bf16[768,256]{1,0:T(8,128)(2,1)} %param.31) | copy-start | bytes 1179652
  81.7 1.0 copy-start.2
  83.9 17.4 %all-to-all-start.2 = ((f32[1,32,4]{2,0,1:T(1,128)}), f32[1,32,4]{2,0,1:T(1,128)S(1)}, u32[]{:S(2)}, u32[]{:S(2)}) async-start(f32[1,32,4]{2,0,1:T(1,128)} %copy.46), calls=%async_computation.2 | async-start | bytes 32768 | tf_op jit(solution)/shard_map/all_to_all | solution.py:158
  89.9 0.7 copy-start.14
  92.1 0.7 copy-start.13
  98.8 1.0 copy-start.7
  101.3 12.6 %all-to-all-start.1 = ((f32[1,32,4]{2,0,1:T(1,128)}), f32[1,32,4]{2,0,1:T(1,128)S(1)}, u32[]{:S(2)}, u32[]{:S(2)}) async-start(f32[1,32,4]{2,0,1:T(1,128)} %copy.43), calls=%async_computation.1 | async-start | bytes 32768 | tf_op jit(solution)/shard_map/all_to_all | solution.py:159
  113.9 10.0 %all-to-all-start = ((f32[1,32,256]{2,0,1:T(1,128)}), f32[1,32,256]{2,0,1:T(1,128)S(1)}, u32[]{:S(2)}, u32[]{:S(2)}) async-start(f32[1,32,256]{2,0,1:T(1,128)} %reshape.442), calls=%async_computation | async-start | bytes 65536 | tf_op jit(solution)/shard_map/all_to_all | solution.py:155
where the time goes:
time: 136 us
  blocking collectives  84.1 us (62%)
  starting transfers between devices  14.8 us (11%)
  local copies, waits for them, and re-layouts  13.7 us (10%)
  waiting for transfers between devices  10.7 us (8%)
  other arithmetic  5.93 us (4%)
  matrix products  4.06 us (3%)
  between operations  2.43 us (2%)
    all_gather x1, blocking collectives, local(): lax.all_gather(piece_rows, 'kv', axis=0, tiled=True)  31.4 us
    all_gather x1, blocking collectives, local(): lax.all_gather(query_lat[:piece_dev], 'kv', axis=0, tiled=True)  30.8 us
    psum x1, blocking collectives, local(): lax.psum(partial_value, 'tp').astype(jnp.float32).astype(jnp.bfloat16)  10.3 us
    all_gather x1, blocking collectives, local(): lax.all_gather(latent_comp, 'tp', axis=1, tiled=True)  6.16 us
    all_to_all x1, starting transfers between devices, local(): lax.all_to_all(local_peak[None], 'kv', split_axis=1, concat_axis=0, tiled...  6 us
    all_to_all x1, waiting for transfers between devices, local(): lax.all_to_all(partial_sum.reshape(1, piece_total, -1), 'kv', split_axis=...  5.73 us
    all_gather x1, blocking collectives, local(): lax.all_gather(query_comp, 'tp', axis=1, tiled=True)  5.5 us
    all_to_all x1, starting transfers between devices, local(): lax.all_to_all(weight_sum[None], 'kv', split_axis=1, concat_axis=0, tiled...  5.43 us
  transfers between devices with their start and end apart: 3, of which 2 were waited for; matrix products, arithmetic and copies ran while one was open for 9% of the time, Pallas kernels for 0%

commit v1 on v0

--- a/solution.py
+++ b/solution.py
@@ -156,7 +156,12 @@
             partial_sum.reshape(1, piece_total, -1), "kv", split_axis=1, concat_axis=0, tiled=True
         ),
         lax.all_to_all(weight_sum[None], "kv", split_axis=1, concat_axis=0, tiled=True),
-        lax.all_to_all(local_peak[None], "kv", split_axis=1, concat_axis=0, tiled=True),
+        jnp.concatenate(
+            lax.all_to_all(
+                jnp.stack(jnp.split(local_peak[None], lax.axis_size("kv"), axis=1)), "kv", 0, 0
+            ),
+            axis=0,
+        ),
     )
     global_peak = jnp.max(all_peaks, axis=0)
     factor = jnp.exp(all_peaks - global_peak[None])

time: 136 us -> 141 us (1.037)
  local copies, waits for them, and re-layouts: 13.7 us -> 18.2 us
    unnamed x40 -> x46, local copies, waits for them, and re-layouts: 5.09 us -> 9.07 us
  transfers between devices with their start and end apart: 3 -> 3, of which waited for: 2 -> 2; matrix products, arithmetic and copies ran while one was open for 9% -> 12% of each run, Pallas kernels for 0% -> 0%
where the time goes in v1:
time: 141 us; the launch traced here: 140 us
  blocking collectives  84.1 us (60%)
  local copies, waits for them, and re-layouts  18.2 us (13%)
  starting transfers between devices  14.8 us (10%)
  waiting for transfers between devices  10.8 us (8%)
  other arithmetic  6.06 us (4%)
  matrix products  4.06 us (3%)
  between operations  2.44 us (2%)
    all_gather x1, blocking collectives, local(): lax.all_gather(piece_rows, 'kv', axis=0, tiled=True)  31.4 us
    all_gather x1, blocking collectives, local(): lax.all_gather(query_lat[:piece_dev], 'kv', axis=0, tiled=True)  30.8 us
    psum x1, blocking collectives, local(): lax.psum(partial_value, 'tp').astype(jnp.float32).astype(jnp.bfloat16)  10.3 us
    unnamed x46, local copies, waits for them, and re-layouts  9.07 us
    all_gather x1, blocking collectives, local(): lax.all_gather(latent_comp, 'tp', axis=1, tiled=True)  6.16 us
    all_to_all x1, starting transfers between devices, local(): lax.all_to_all(jnp.stack(jnp.split(local_peak[None], lax.axis_size('kv'),...  6.01 us
    all_to_all x1, waiting for transfers between devices, local(): lax.all_to_all(partial_sum.reshape(1, piece_total, -1), 'kv', split_axis=...  5.85 us
    all_gather x1, blocking collectives, local(): lax.all_gather(query_comp, 'tp', axis=1, tiled=True)  5.5 us
  transfers between devices with their start and end apart: 3, of which 2 were waited for; matrix products, arithmetic and copies ran while one was open for 12% of the time, Pallas kernels for 0%

profile of v1, /device:TPU:0, one launch (start us, length us, event | category | flops | bytes accessed | tf_op | source)
XLA Modules:
  0.0 140.5 jit_solution(11163216246703736530)
XLA Ops:
  0.7 1.3 copy.113
  4.0 6.2 %all_gather.14 = bf16[5,512]{1,0:T(8,128)(2,1)S(1)} all-gather(bf16[5,128]{1,0:T(8,128)(2,1)S(1)} %convolution_convert_fusion.5), channel_id=1, replica_groups=mesh['kv'=8,'tp'=4] {'tp'}, dimensions={1}, use_global_device_ids=true | all-gather | bytes 6400 | tf_op jit(solution)/shard_map/all_gather | solution.py:122
  10.6 5.5 %all-gather = bf16[4,192,5]{1,2,0:T(8,128)(2,1)S(1)} all-gather(bf16[1,192,5]{1,2,0:T(8,128)(2,1)S(1)} %fusion.5), channel_id=1, replica_groups=mesh['kv'=8,'tp'=4] {'tp'}, dimensions={0}, use_global_device_ids=true | all-gather | bytes 9600 | tf_op jit(solution)/shard_map/all_gather | solution.py:121
  17.6 31.4 %all-gather.2 = bf16[8,4,544]{2,1,0:T(4,128)(2,1)S(1)} all-gather(bf16[1,4,544]{2,1,0:T(4,128)(2,1)S(1)} %slice_bitcast_fusion.14), channel_id=1, replica_groups=mesh['kv'=8,'tp'=4] {'kv'}, dimensions={0}, use_global_device_ids=true | all-gather | bytes 39168 | tf_op jit(solution)/shard_map/all_gather | solution.py:136
  49.2 30.8 %all-gather.1 = bf16[8,4,768]{2,1,0:T(4,128)(2,1)S(1)} all-gather(bf16[1,4,768]{2,1,0:T(4,128)(2,1)S(1)} %slice_bitcast_fusion.10), channel_id=1, replica_groups=mesh['kv'=8,'tp'=4] {'kv'}, dimensions={0}, use_global_device_ids=true | all-gather | bytes 55296 | tf_op jit(solution)/shard_map/all_gather | solution.py:135
  80.9 0.9 fusion.10
  81.9 0.7 copy-done.2
  83.2 0.7 copy.73
  83.9 5.4 %all-to-all-start.2 = ((f32[1,32,4]{2,0,1:T(1,128)}), f32[1,32,4]{2,0,1:T(1,128)S(1)}, u32[]{:S(2)}, u32[]{:S(2)}) async-start(f32[1,32,4]{2,0,1:T(1,128)} %copy.73), calls=%async_computation.2 | async-start | bytes 32768 | tf_op jit(solution)/shard_map/all_to_all | solution.py:158
  89.9 0.6 copy-done.14
  91.3 0.8 constant_dynamic-slice_fusion
  92.1 0.7 copy-done.13
  92.8 2.0 %and_reduce_fusion = pred[]{:T(512)} fusion(s32[3]{0:T(128)S(1)} %copy-done.13, s32[1]{0:T(128)} %bitcast.28, s32[1]{0:T(128)} %bitcast.27, s32[1]{0:T(128)} %constant.79.clone.1), kind=kLoop, calls=%fused_computation.117 | loop fusion | flops 17 | bytes 25 | tf_op jit(solution)/shard_map/reduce.1
  94.8 1.2 broadcast_select_fusion
  96.2 1.6 %scatter.4 = bf16[1,768,544]{1,2,0:T(8,128)(2,1)S(1)} dynamic-update-slice(bf16[1,768,544]{1,2,0:T(8,128)(2,1)S(1)} %copy.113, bf16[1,1,544]{1,2,0:T(8,128)(2,1)S(1)} %copy.77, s32[]{:T(128)} %constant.75.clone.1, s32[]{:T(128)} %bitcast.30, s32[]{:T(128)} %constant.75.clone.1) | dynamic-update-slice | bytes 2180 | tf_op jit(solution)/shard_map/vmap(vmap())/scatter | solution.py:84
  99.1 0.6 copy-done.7
  106.1 6.0 %all-to-all-start.1 = ((f32[8,1,4,4]{3,2,1,0:T(4,128)}), f32[8,1,4,4]{3,2,1,0:T(4,128)S(1)}, u32[]{:S(2)}, u32[]{:S(2)}) async-start(f32[8,1,4,4]{3,2,1,0:T(4,128)} %constant_dynamic-update-slice_fusion), calls=%async_computation.1 | async-start | bytes 32768 | tf_op jit(solution)/shard_map/all_to_all | solution.py:160
  112.9 0.7 reshape.446
  113.7 5.0 %all-to-all-done.1 = f32[8,1,4,4]{3,2,1,0:T(4,128)S(1)} async-done(((f32[8,1,4,4]{3,2,1,0:T(4,128)}), f32[8,1,4,4]{3,2,1,0:T(4,128)S(1)}, u32[]{:S(2)}, u32[]{:S(2)}) %all-to-all-start.1) | async-done | bytes 544 | tf_op jit(solution)/shard_map/all_to_all | solution.py:160
  118.7 3.3 %all-to-all-start = ((f32[1,32,256]{2,0,1:T(1,128)}), f32[1,32,256]{2,0,1:T(1,128)S(1)}, u32[]{:S(2)}, u32[]{:S(2)}) async-start(f32[1,32,256]{2,0,1:T(1,128)} %reshape.446), calls=%async_computation | async-start | bytes 65536 | tf_op jit(solution)/shard_map/all_to_all | solution.py:155
  122.8 5.8 %all-to-all-done = f32[1,32,256]{2,0,1:T(1,128)S(1)} async-done(((f32[1,32,256]{2,0,1:T(1,128)}), f32[1,32,256]{2,0,1:T(1,128)S(1)}, u32[]{:S(2)}, u32[]{:S(2)}) %all-to-all-start) | async-done | bytes 32800 | tf_op jit(solution)/shard_map/all_to_all | solution.py:155
  129.0 10.3 %psum.7 = bf16[5,2048]{1,0:T(8,128)(2,1)S(1)} all-reduce(bf16[5,2048]{1,0:T(8,128)(2,1)S(1)} %convolution_convert_fusion), channel_id=1, replica_groups=mesh['kv'=8,'tp'=4] {'tp'}, use_global_device_ids=true, to_apply=%region_11.12 | all-reduce | flops 10240 | bytes 40960 | tf_op jit(solution)/shard_map/psum | solution.py:188
  139.3 0.6 slice.104
  139.9 0.6 slice.105
  (121 shorter events, 15.3 us)
Async XLA Ops:
  0.6 128.1 %copy-start = (bf16[256,2048]{1,0:T(8,128)(2,1)S(1)}, bf16[256,2048]{1,0:T(8,128)(2,1)}, u32[]{:S(2)}) copy-start(bf16[256,2048]{1,0:T(8,128)(2,1)} %param.35) | copy-start | bytes 3145732
  0.6 3.1 %copy-start.5 = (bf16[2048,128]{1,0:T(8,128)(2,1)S(1)}, bf16[2048,128]{1,0:T(8,128)(2,1)}, u32[]{:S(2)}) copy-start(bf16[2048,128]{1,0:T(8,128)(2,1)} %param.29) | copy-start | bytes 1572868
  0.7 2.9 %copy-start.15 = (bf16[2048,32]{0,1:T(8,128)(2,1)S(1)}, bf16[2048,32]{0,1:T(8,128)(2,1)}, u32[]{:S(2)}) copy-start(bf16[2048,32]{0,1:T(8,128)(2,1)} %param.30) | copy-start | bytes 393220
  0.7 2.7 %copy-start.8 = (bf16[4,2048]{1,0:T(4,128)(2,1)S(1)}, bf16[4,2048]{1,0:T(4,128)(2,1)}, u32[]{:S(2)}) copy-start(bf16[4,2048]{1,0:T(4,128)(2,1)} %param.19) | copy-start | bytes 49156
  0.7 2.7 %copy-start.9 = (bf16[1,2048]{1,0:T(2,128)(2,1)S(1)}, bf16[1,2048]{1,0:T(2,128)(2,1)}, u32[]{:S(2)}) copy-start(bf16[1,2048]{1,0:T(2,128)(2,1)} %param.20) | copy-start | bytes 12292
  0.7 2.9 %copy-start.10 = (f32[2048]{0:T(1024)S(1)}, f32[2048]{0:T(1024)}, u32[]{:S(2)}) copy-start(f32[2048]{0:T(1024)} %param.25) | copy-start | bytes 24580
  2.0 8.3 %copy-start.3 = (bf16[2048,192]{0,1:T(8,128)(2,1)S(1)}, bf16[2048,192]{0,1:T(8,128)(2,1)}, u32[]{:S(2)}) copy-start(bf16[2048,192]{0,1:T(8,128)(2,1)} %param.28) | copy-start | bytes 2359300
  10.3 6.1 %copy-start.6 = (bf16[256,544]{0,1:T(8,128)(2,1)S(1)}, bf16[256,544]{0,1:T(8,128)(2,1)}, u32[]{:S(2)}) copy-start(bf16[256,544]{0,1:T(8,128)(2,1)} %param.23) | copy-start | bytes 835588
  16.6 0.7 copy-start.12
  17.3 31.8 %copy-start.11 = (f32[768]{0:T(1024)S(1)}, f32[768]{0:T(1024)}, u32[]{:S(2)}) copy-start(f32[768]{0:T(1024)} %param.26) | copy-start | bytes 9220
  17.5 62.5 %copy-start.4 = (bf16[768,128]{1,0:T(8,128)(2,1)S(1)}, bf16[768,128]{1,0:T(8,128)(2,1)}, u32[]{:S(2)}) copy-start(bf16[768,128]{1,0:T(8,128)(2,1)} %param.32) | copy-start | bytes 589828
  17.5 62.8 %copy-start.1 = (bf16[768,256]{1,0:T(8,128)(2,1)S(1)}, bf16[768,256]{1,0:T(8,128)(2,1)}, u32[]{:S(2)}) copy-start(bf16[768,256]{1,0:T(8,128)(2,1)} %param.31) | copy-start | bytes 1179652
  81.7 1.0 copy-start.2
  83.9 22.2 %all-to-all-start.2 = ((f32[1,32,4]{2,0,1:T(1,128)}), f32[1,32,4]{2,0,1:T(1,128)S(1)}, u32[]{:S(2)}, u32[]{:S(2)}) async-start(f32[1,32,4]{2,0,1:T(1,128)} %copy.73), calls=%async_computation.2 | async-start | bytes 32768 | tf_op jit(solution)/shard_map/all_to_all | solution.py:158
  89.9 0.7 copy-start.14
  92.1 0.7 copy-start.13
  98.8 1.0 copy-start.7
  106.1 12.6 %all-to-all-start.1 = ((f32[8,1,4,4]{3,2,1,0:T(4,128)}), f32[8,1,4,4]{3,2,1,0:T(4,128)S(1)}, u32[]{:S(2)}, u32[]{:S(2)}) async-start(f32[8,1,4,4]{3,2,1,0:T(4,128)} %constant_dynamic-update-slice_fusion), calls=%async_computation.1 | async-start | bytes 32768 | tf_op jit(solution)/shard_map/all_to_all | solution.py:160
  118.7 10.0 %all-to-all-start = ((f32[1,32,256]{2,0,1:T(1,128)}), f32[1,32,256]{2,0,1:T(1,128)S(1)}, u32[]{:S(2)}, u32[]{:S(2)}) async-start(f32[1,32,256]{2,0,1:T(1,128)} %reshape.446), calls=%async_computation | async-start | bytes 65536 | tf_op jit(solution)/shard_map/all_to_all | solution.py:155
